TPU v7x, 256 devices: a whole 4x4x8 slice. The times are simulated.
256 devices in a mesh: sp: 16 (over y, x), tp: 16 (over z, core).
Axes of the slice: x: 4, y: 4, z: 8, core: 2. Of those that a mesh axis runs over, the one named last changes fastest.
Arguments:
- queries: bfloat16 [16384, 1536], P('sp', 'tp'), may hold values from -34 to 34
- latent: bfloat16 [16384, 512], P('sp'), may hold values from -6 to 6
- rot_key: bfloat16 [16384, 32], P('sp'), may hold values from -34 to 34
- latent_gain: float32 [512], replicated, may hold values from 0.1 to 1.9
- key_up: bfloat16 [512, 1024], P(None, 'tp'), may hold values from -0.25 to 0.25
- value_up: bfloat16 [512, 1024], P(None, 'tp'), may hold values from -0.70710678 to 0.70710678
- query_gain: float32 [96], replicated, may hold values from 0.5 to 6
- key_gain: float32 [96], replicated, may hold values from 0.5 to 6
- out_gain: float32 [1024], replicated, may hold values from 0.1 to 1.9
- out_weight: bfloat16 [1024, 2048], replicated, may hold values from -0.1875 to 0.1875
- residual: bfloat16 [16384, 2048], P(('sp', 'tp')), may hold values from -6 to 6
- ffn_gain: float32 [2048], replicated, may hold values from 0.1 to 1.9
- routes: int32 [16384, 2], P(('sp', 'tp')), may hold values from 0 to 15, all different within a row; in each aligned block of 64 rows (0 to 63, 64 to 127, ...) at most 9 rows name the same one
- route_weights: float32 [16384, 2], P(('sp', 'tp')), may hold values from 0.2 to 1
- expert_gate: bfloat16 [16, 2048, 2048], P('sp', None, 'tp'), may hold values from -0.125 to 0.125
- expert_up: bfloat16 [16, 2048, 2048], P('sp', None, 'tp'), may hold values from -0.125 to 0.125
- expert_down: bfloat16 [16, 2048, 2048], P('sp', 'tp'), may hold values from -0.125 to 0.125
Outputs:
- layer_out: bfloat16 [16384, 2048], P(('sp', 'tp'))
Inputs may be any that keep to these rules, and one draw needn't show every extreme that they name: `routes`: the 2 experts of a token differ. Among the 64 rows of one device each expert is named by at most 9 rows, a bound that some block reaches.
All inputs are finite; a program needn't handle non-finite values.
Results may differ from a plain program's by a relative error of at most 0.02.
The roundings to bfloat16 on the way count: a program that leaves them out, or rounds other values in their place, can miss the bound.
Values may be sent and summed in bfloat16 or wider, within the bound.
A program may use at most 128 MiB of HBM per device.

v0:
```python
import jax
import jax.numpy as jnp
from jax import lax
from jax.sharding import PartitionSpec as P

D = 2048
NOPE = 64
ROPE = 32
VH = 64
TOPK = 2
QK = 96
epsilon = 1e-06
rope_base = 10000.0


def rms_scale(values):
    return lax.rsqrt(jnp.mean(values * values, axis=-1, keepdims=True) + epsilon)


def rotate_half(values, angles):
    half_dims = values.shape[-1] // 2
    first_half = values[..., :half_dims]
    second_half = values[..., half_dims:]
    cosine = jnp.cos(angles)
    sine_val = jnp.sin(angles)
    return jnp.concatenate(
        [
            first_half * cosine - second_half * sine_val,
            second_half * cosine + first_half * sine_val,
        ],
        axis=-1,
    )


def head_prepare(raw_rows, gain_vec, angles):
    normed_rows = raw_rows * rms_scale(raw_rows) * gain_vec
    turned_rows = rotate_half(normed_rows[..., NOPE:], angles[:, None, :])
    return jnp.concatenate([normed_rows[..., :NOPE], turned_rows], axis=-1).astype(jnp.bfloat16)


def slot_targets(route_rows, expert_total, slot_cap):
    flat_routes = route_rows.reshape(-1)
    one_hot = (flat_routes[:, None] == jnp.arange(expert_total, dtype=jnp.int32)[None, :]).astype(
        jnp.int32
    )
    earlier = jnp.cumsum(one_hot, axis=0) - one_hot
    rank_in = jnp.sum(earlier * one_hot, axis=1)
    return (flat_routes * slot_cap + rank_in).reshape(route_rows.shape)


def select_matrix(targets, slot_total):
    hits = targets[:, :, None] == jnp.arange(slot_total, dtype=jnp.int32)[None, None, :]
    return jnp.sum(hits.astype(jnp.bfloat16), axis=1)


def shards(
    queries,
    latent,
    rot_key,
    latent_gain,
    key_up,
    value_up,
    query_gain,
    key_gain,
    out_gain,
    out_weight,
    residual,
    ffn_gain,
    routes,
    route_weights,
    expert_gate,
    expert_up,
    expert_down,
):
    shard_len = queries.shape[0]
    local_heads = key_up.shape[1] // NOPE
    sp_count = lax.axis_size("sp")
    tp_count = lax.axis_size("tp")
    my_first = lax.axis_index("sp") * shard_len
    my_last = my_first + shard_len - 1
    positions = my_first + jnp.arange(shard_len, dtype=jnp.int32)
    inverse = rope_base ** (-jnp.arange(0, ROPE, 2, dtype=jnp.float32) / ROPE)
    angles = positions.astype(jnp.float32)[:, None] * inverse[None, :]
    lat_f32 = latent.astype(jnp.float32)
    normed_latent = (lat_f32 * rms_scale(lat_f32) * latent_gain).astype(jnp.bfloat16)
    key_nope = jnp.dot(normed_latent, key_up, preferred_element_type=jnp.float32).astype(
        jnp.bfloat16
    )
    value_rows = jnp.dot(normed_latent, value_up, preferred_element_type=jnp.float32).astype(
        jnp.bfloat16
    )
    shared = rot_key.astype(jnp.float32)[:, None, :]
    raw_keys = jnp.concatenate(
        [key_nope.astype(jnp.float32).reshape(shard_len, local_heads, NOPE), shared], axis=-1
    )
    key_rows = head_prepare(raw_keys, key_gain, angles)
    query_rows = head_prepare(
        queries.astype(jnp.float32).reshape(shard_len, local_heads, QK), query_gain, angles
    )
    query_heads = jnp.transpose(query_rows, (1, 0, 2))
    bundle = jnp.concatenate(
        [
            jnp.transpose(key_rows, (1, 2, 0)),
            jnp.transpose(value_rows.reshape(shard_len, local_heads, VH), (1, 2, 0)),
        ],
        axis=1,
    )
    score_scale = QK ** (-0.5)
    init_state = (
        jnp.full((local_heads, shard_len), -1e30, jnp.float32),
        jnp.zeros((local_heads, shard_len), jnp.float32),
        jnp.zeros((local_heads, shard_len, VH), jnp.float32),
    )
    key_piece = lax.all_gather(bundle, "sp", axis=2, tiled=True)
    block_count = key_piece.shape[2] // shard_len

    def one_block(block_index, running_state):
        first_key = block_index * shard_len

        def compute(inner):
            row_peak, row_total, weighted = inner
            key_part = lax.dynamic_slice_in_dim(key_piece, block_index * shard_len, shard_len, 2)
            scores = (
                jnp.einsum(
                    "hqc,hck->hqk",
                    query_heads,
                    key_part[:, :QK, :],
                    preferred_element_type=jnp.float32,
                )
                * score_scale
            )
            key_pos = first_key + jnp.arange(shard_len, dtype=jnp.int32)
            allowed = key_pos[None, None, :] <= positions[None, :, None]
            scores = jnp.where(allowed, scores, -1e30)
            new_peak = jnp.maximum(row_peak, jnp.max(scores, axis=2))
            exponent = jnp.where(allowed, jnp.exp(scores - new_peak[..., None]), 0.0)
            factor = jnp.exp(row_peak - new_peak)
            new_total = row_total * factor + jnp.sum(exponent, axis=2)
            contrib = jnp.einsum(
                "hqk,hvk->hqv",
                exponent.astype(jnp.bfloat16),
                key_part[:, QK:, :],
                preferred_element_type=jnp.float32,
            )
            return (new_peak, new_total, weighted * factor[..., None] + contrib)

        return lax.cond(first_key <= my_last, compute, lambda inner: inner, running_state)

    row_peak, row_total, weighted = lax.fori_loop(0, block_count, one_block, init_state)
    attended = (weighted / row_total[..., None]).astype(jnp.bfloat16)
    tok_count = residual.shape[0]
    head_major = jnp.transpose(attended, (1, 0, 2)).reshape(shard_len, local_heads * VH)
    token_rows = lax.all_to_all(head_major, "tp", split_axis=0, concat_axis=1, tiled=True).astype(
        jnp.float32
    )
    normed_rows = (token_rows * rms_scale(token_rows) * out_gain).astype(jnp.bfloat16)
    partials = jnp.einsum(
        "tgc,gcd->tgd",
        normed_rows.reshape(tok_count, tp_count, -1),
        out_weight.reshape(tp_count, -1, D),
        preferred_element_type=jnp.float32,
    )
    rounded = lax.optimization_barrier(partials.astype(jnp.bfloat16))
    mixed = jnp.sum(rounded.astype(jnp.float32), axis=1)
    middle = residual.astype(jnp.float32) + mixed
    ffn_input = (middle * rms_scale(middle) * ffn_gain).astype(jnp.bfloat16)
    slot_cap = max(2, 9 * tok_count * TOPK // (8 * sp_count))
    slot_total = sp_count * slot_cap
    targets = slot_targets(routes, sp_count, slot_cap)
    chooser = select_matrix(targets, slot_total)
    outbound = (
        jnp.einsum("ts,td->sd", chooser, ffn_input, preferred_element_type=jnp.float32)
        .astype(jnp.bfloat16)
        .reshape(sp_count, slot_cap, D)
    )
    arrived = lax.all_to_all(outbound, "sp", split_axis=0, concat_axis=0, tiled=True)
    item_count = arrived.shape[1]
    flat_rows = arrived.reshape(sp_count * item_count, D)
    row_block = lax.all_gather(flat_rows, "tp", axis=0, tiled=True)
    gate_pre = jnp.dot(row_block, expert_gate[0], preferred_element_type=jnp.float32)
    up_pre = jnp.dot(row_block, expert_up[0], preferred_element_type=jnp.float32)
    hidden = (jax.nn.silu(gate_pre) * up_pre).astype(jnp.bfloat16)
    served = lax.psum_scatter(
        jnp.dot(hidden, expert_down[0], preferred_element_type=jnp.float32).astype(jnp.bfloat16),
        "tp",
        scatter_dimension=0,
        tiled=True,
    ).reshape(sp_count, item_count, D)
    returned_rows = lax.all_to_all(served, "sp", split_axis=0, concat_axis=0, tiled=True).reshape(
        slot_total, D
    )
    picked = (
        jnp.take(returned_rows, targets.reshape(-1), axis=0)
        .reshape(tok_count, TOPK, D)
        .astype(jnp.float32)
    )
    moe_sum = jnp.sum(picked * route_weights[:, :, None], axis=1)
    return (middle + moe_sum).astype(jnp.bfloat16)


def solution(mesh):
    return jax.shard_map(
        shards,
        mesh=mesh,
        in_specs=(
            P("sp", "tp"),
            P("sp", None),
            P("sp", None),
            P(),
            P(None, "tp"),
            P(None, "tp"),
            P(),
            P(),
            P(),
            P(),
            P(("sp", "tp"), None),
            P(),
            P(("sp", "tp"), None),
            P(("sp", "tp"), None),
            P("sp", None, "tp"),
            P("sp", None, "tp"),
            P("sp", "tp", None),
        ),
        out_specs=P(("sp", "tp"), None),
        check_vma=False,
    )
```

profile of v0, /device:TPU:97, one launch (start us, length us, event | category | flops | bytes accessed | tf_op | source)
XLA Modules:
  0.0 451.1 jit_solution(6509418621641927697)
XLA Ops:
  6.6 1.6 fusion.21
  8.3 1.8 fusion.29
  10.1 0.9 fusion.40
  11.0 1.0 fusion.42
  12.0 1.0 fusion.41
  13.0 0.6 fusion.30
  13.7 0.3 fusion.74
  14.1 0.7 pad_maximum_fusion
  14.9 0.2 copy.34
  15.2 0.1 reshape.499
  15.5 0.2 reduce_window_sum.11
  15.7 0.2 select_reduce_fusion
  15.8 0.1 reduce_sum.105
  16.1 61.9 %all-gather.3.cloned.1.call-done = bf16[1,160,16384]{2,1,0:T(8,128)(2,1)} async-done(((bf16[1,160,1024]{2,1,0:T(8,128)(2,1)}), bf16[1,160,16384]{2,1,0:T(8,128)(2,1)}) %all-gather.3.cloned.1.call-update) | async-done | bytes 5242896 | tf_op jit(solution)/shard_map/all_gather | solution.py:114
  78.0 9.9 %while.18 = (s32[]{:T(128)}, f32[1,1024]{1,0:T(1,128)S(1)}, f32[1,1024]{1,0:T(1,128)S(1)}, f32[1,1024,64]{1,2,0:T(8,128)S(1)}, s32[]{:T(128)}, /*index=5*/bf16[1...) while((s32[]{:T(128)}, f32[1,1024]{1,0:T(1,128)S(1)}, ...), condition=%wide.region_8.9_spmd.clone, body=%wide.region_3.8_spmd.clone.sunk | while | flops 352456704 | bytes 30515560 | solution.py:149
  78.0 9.1 %conditional.3 = ((f32[1,1024]{1,0:T(1,128)S(1)}, f32[1,1024]{1,0:T(1,128)S(1)}, f32[1,1024,64]{1,2,0:T(8,128)S(1)})) conditional(s32[]{:T(128)} %convert_element_type.207, (f32[1,1024]{1,0:T(1,128)S(1)}, f32[1,1024]{1,0:T(1,128)S(1)}, f32[1,1024,64]{1,2,0:T(8,128)S(1)}) %tuple.54, (s32[]{:T(128)}, s32[]{:T(128)}, s32[]{:T(128)}, ...), branch_computations={%region_4.0_spmd, %region_5.7_spmd} | conditional | flops 352456704 | bytes 30511242 | solution.py:147
  78.0 2.0 fusion.2
  80.1 2.0 copy-done.1
  82.1 1.5 fusion.4
  83.7 3.5 fusion.10
  87.9 0.2 copy.41
  88.1 0.9 reshape.512
  89.0 7.8 %all-to-all-start = ((bf16[16,2,2048]{2,1,0:T(2,128)(2,1)}), bf16[16,2,2048]{2,1,0:T(2,128)(2,1)S(1)}, u32[]{:S(2)}, u32[]{:S(2)}) async-start(bf16[16,2,2048]{2,1,0:T(2,128)(2,1)} %reshape.512), calls=%async_computation | async-start | bytes 262144 | tf_op jit(solution)/shard_map/all_to_all | solution.py:153
  96.9 6.2 %all-to-all-done = bf16[16,2,2048]{2,1,0:T(2,128)(2,1)S(1)} async-done(((bf16[16,2,2048]{2,1,0:T(2,128)(2,1)}), bf16[16,2,2048]{2,1,0:T(2,128)(2,1)S(1)}, u32[]{:S(2)}, u32[]{:S(2)}) %all-to-all-start) | async-done | bytes 131104 | tf_op jit(solution)/shard_map/all_to_all | solution.py:153
  103.1 0.2 reshape.513
  103.3 0.2 fusion.32
  103.5 3.5 convert_bitcast_fusion
  107.1 0.8 convert_reduce_fusion
  107.8 0.2 copy-done.2
  108.0 0.2 multiply_reduce_fusion.1
  108.2 0.4 convolution_convert_fusion.1
  108.5 0.2 reshape.500
  108.8 156.9 %all_to_all.23 = bf16[16,9,2048]{2,1,0:T(8,128)(2,1)S(1)} all-to-all(bf16[16,9,2048]{2,1,0:T(8,128)(2,1)S(1)} %reshape.500), channel_id=1, replica_groups=mesh['sp'=16,'tp'=16] {'sp'}, dimensions={0} | all-to-all | bytes 1179648 | tf_op jit(solution)/shard_map/all_to_all | solution.py:176
  265.7 1.1 reshape.501
  266.8 0.2 reduce-scatter.2.cloned.1.call-start
  267.1 57.2 %all-gather.5.cloned.1.call-done = bf16[2304,2048]{1,0:T(8,128)(2,1)} async-done(((bf16[144,2048]{1,0:T(8,128)(2,1)}), bf16[2304,2048]{1,0:T(8,128)(2,1)}) %all-gather.5.cloned.1.call-update) | async-done | bytes 9437200 | tf_op jit(solution)/shard_map/all_gather | solution.py:179
  324.3 5.3 %fusion.38 = f32[2304,128]{1,0:T(8,128)S(1)} fusion(bf16[2304,2048]{1,0:T(8,128)(2,1)} %all-gather.5.cloned.1.call-done, bf16[1,2048,128]{2,1,0:T(8,128)(2,1)} %param.35), kind=kOutput, calls=%fused_computation.53 | convolution fusion | flops 1207959552 | bytes 11141120 | tf_op jit(solution)/shard_map/dot_general | solution.py:180
  329.6 14.2 %convolution_convert_fusion = bf16[2304,2048]{1,0:T(8,128)(2,1)} fusion(bf16[2304,2048]{1,0:T(8,128)(2,1)} %all-gather.5.cloned.1.call-done, f32[2304,128]{1,0:T(8,128)S(1)} %fusion.38, bf16[1,128,2048]{2,1,0:T(8,128)(2,1)S(1)} %copy-done, bf16[1,2048,128]{2,1,0:T(8,128)(2,1)S(1)} %copy-done.5), kind=kOutput, calls=%fused_computation.23 | convolution fusion | flops 2422407168 | bytes 21102592 | tf_op jit(solution)/shard_map/dot_general | solution.py:184
  343.9 71.6 %reduce-scatter.2.cloned.1.call-done = bf16[144,2048]{1,0:T(8,128)(2,1)} async-done(((bf16[2304,2048]{1,0:T(8,128)(2,1)}), bf16[144,2048]{1,0:T(8,128)(2,1)}) %reduce-scatter.2.cloned.1.call-update) | async-done | bytes 589840 | tf_op jit(solution)/shard_map/reduce_scatter | solution.py:183
  415.5 2.3 reshape.502
  417.8 6.5 %all-to-all-start.2 = ((bf16[16,9,2048]{2,1,0:T(8,128)(2,1)}), bf16[16,9,2048]{2,1,0:T(8,128)(2,1)S(1)}, u32[]{:S(2)}, u32[]{:S(2)}) async-start(bf16[16,9,2048]{2,1,0:T(8,128)(2,1)} %reshape.502), calls=%async_computation.3 | async-start | bytes 2097152 | tf_op jit(solution)/shard_map/all_to_all | solution.py:189
  424.4 0.1 mul.304
  424.8 15.1 %all-to-all-done.2 = bf16[16,9,2048]{2,1,0:T(8,128)(2,1)S(1)} async-done(((bf16[16,9,2048]{2,1,0:T(8,128)(2,1)}), bf16[16,9,2048]{2,1,0:T(8,128)(2,1)S(1)}, u32[]{:S(2)}, u32[]{:S(2)}) %all-to-all-start.2) | async-done | bytes 589856 | tf_op jit(solution)/shard_map/all_to_all | solution.py:189
  439.9 0.3 reshape.503
  440.2 0.9 gather_fusion
  441.1 0.3 gather.7
  441.4 2.3 multiply_reduce_fusion
  443.8 0.8 add_convert_fusion
  (92 shorter events, 1.4 us)
Async XLA Ops:
  6.5 323.1 %copy-start = (bf16[1,128,2048]{2,1,0:T(8,128)(2,1)S(1)}, bf16[1,128,2048]{2,1,0:T(8,128)(2,1)}, u32[]{:S(2)}) copy-start(bf16[1,128,2048]{2,1,0:T(8,128)(2,1)} %param.37) | copy-start | bytes 1572868
  6.5 6.4 %copy-start.3 = (bf16[1024,512]{1,0:T(8,128)(2,1)S(1)}, bf16[1024,512]{1,0:T(8,128)(2,1)}, u32[]{:S(2)}) copy-start(bf16[1024,512]{1,0:T(8,128)(2,1)} %param.22) | copy-start | bytes 3145732
  6.5 6.5 %copy-start.12 = (f32[512]{0:T(512)S(1)}, f32[512]{0:T(512)}, u32[]{:S(2)}) copy-start(f32[512]{0:T(512)} %param.24) | copy-start | bytes 6148
  6.5 7.0 %copy-start.4 = (bf16[1024,96]{0,1:T(8,128)(2,1)S(1)}, bf16[1024,96]{0,1:T(8,128)(2,1)}, u32[]{:S(2)}) copy-start(bf16[1024,96]{0,1:T(8,128)(2,1)} %param.21) | copy-start | bytes 589828
  6.5 6.5 %copy-start.11 = (bf16[512,64]{0,1:T(8,128)(2,1)S(1)}, bf16[512,64]{0,1:T(8,128)(2,1)}, u32[]{:S(2)}) copy-start(bf16[512,64]{0,1:T(8,128)(2,1)} %param.26) | copy-start | bytes 196612
  6.5 7.0 %copy-start.10 = (f32[96]{0:T(128)S(1)}, f32[96]{0:T(128)}, u32[]{:S(2)}) copy-start(f32[96]{0:T(128)} %param.27) | copy-start | bytes 1156
  6.6 71.4 %all-gather.3.cloned.1.call-start = ((), (), s32[]{:S(2)}) async-start(), calls=%async_computation.4 | async-start | bytes 5570560 | tf_op jit(solution)/shard_map/all_gather | solution.py:114
  8.3 6.8 %copy-start.8 = (f32[1024]{0:T(1024)S(1)}, f32[1024]{0:T(1024)}, u32[]{:S(2)}) copy-start(f32[1024]{0:T(1024)} %param.29) | copy-start | bytes 12292
  8.3 6.9 %copy-start.6 = (s32[64,2]{0,1:T(2,128)S(1)}, s32[64,2]{0,1:T(2,128)}, u32[]{:S(2)}) copy-start(s32[64,2]{0,1:T(2,128)} %param.33) | copy-start | bytes 1540
  80.1 2.0 copy-start.1
  89.0 14.1 %all-to-all-start = ((bf16[16,2,2048]{2,1,0:T(2,128)(2,1)}), bf16[16,2,2048]{2,1,0:T(2,128)(2,1)S(1)}, u32[]{:S(2)}, u32[]{:S(2)}) async-start(bf16[16,2,2048]{2,1,0:T(2,128)(2,1)} %reshape.512), calls=%async_computation | async-start | bytes 262144 | tf_op jit(solution)/shard_map/all_to_all | solution.py:153
  96.8 227.5 %all-gather.5.cloned.1.call-start = ((), (), s32[]{:S(2)}) async-start(), calls=%async_computation.5 | async-start | bytes 10027008 | tf_op jit(solution)/shard_map/all_gather | solution.py:179
  107.0 1.0 copy-start.2
  107.0 1.1 copy-start.7
  266.8 62.8 %copy-start.5 = (bf16[1,2048,128]{2,1,0:T(8,128)(2,1)S(1)}, bf16[1,2048,128]{2,1,0:T(8,128)(2,1)}, u32[]{:S(2)}) copy-start(bf16[1,2048,128]{2,1,0:T(8,128)(2,1)} %param.36) | copy-start | bytes 1572868
  266.8 148.7 %reduce-scatter.2.cloned.1.call-start = ((), (), s32[]{:S(2)}) async-start(), calls=%async_computation.6 | async-start | bytes 10027008 | tf_op jit(solution)/shard_map/reduce_scatter | solution.py:183
  343.8 80.8 %copy-start.9 = (f32[64,2]{0,1:T(2,128)S(1)}, f32[64,2]{0,1:T(2,128)}, u32[]{:S(2)}) copy-start(f32[64,2]{0,1:T(2,128)} %param.34) | copy-start | bytes 1540
  417.8 22.1 %all-to-all-start.2 = ((bf16[16,9,2048]{2,1,0:T(8,128)(2,1)}), bf16[16,9,2048]{2,1,0:T(8,128)(2,1)S(1)}, u32[]{:S(2)}, u32[]{:S(2)}) async-start(bf16[16,9,2048]{2,1,0:T(8,128)(2,1)} %reshape.502), calls=%async_computation.3 | async-start | bytes 2097152 | tf_op jit(solution)/shard_map/all_to_all | solution.py:189
Sparse Core Ops, SparseCore 0:
  14.9 62.9 all-gather.2
  266.9 57.2 all-gather.4
  344.0 71.4 reduce-scatter.1
where the time goes:
time: 452 us; the launch traced here: 451 us
  waiting for transfers between devices  212 us (47%)
  blocking collectives  157 us (35%)
  matrix products  31.3 us (7%)
  starting transfers between devices  14.6 us (3%)
  between operations  13.5 us (3%)
  other arithmetic  12 us (3%)
  local copies, waits for them, and re-layouts  9.85 us (2%)
    all_to_all x1, blocking collectives, shards(): lax.all_to_all(outbound, 'sp', split_axis=0, concat_axis=0, tiled=True)  157 us
    reduce_scatter x1, waiting for transfers between devices, shards(): lax.psum_scatter(jnp.dot(hidden, expert_down[0], preferred_element_type=j...  71.6 us
    all_gather x1, waiting for transfers between devices, shards(): key_piece = lax.all_gather(bundle, 'sp', axis=2, tiled=True)  61.9 us
    all_gather x1, waiting for transfers between devices, shards(): row_block = lax.all_gather(flat_rows, 'tp', axis=0, tiled=True)  57.2 us
    all_to_all x1, waiting for transfers between devices, shards(): lax.all_to_all(served, 'sp', split_axis=0, concat_axis=0, tiled=True)  15.1 us
    dot_general x1, matrix products, shards(): jnp.dot(hidden, expert_down[0], preferred_element_type=jnp.float32)  14.2 us
  transfers between devices with their start and end apart: 5, of which 5 were waited for; matrix products, arithmetic and copies ran while one was open for 0% of the time, Pallas kernels for 0%

commit v1 on v0

--- a/solution.py
+++ b/solution.py
@@ -11,6 +11,11 @@
 QK = 96
 epsilon = 1e-06
 rope_base = 10000.0
+
+
+def exchange_gather(x, mesh_axis, dim):
+    outgoing = jnp.stack([x] * lax.axis_size(mesh_axis))
+    return jnp.concatenate(lax.all_to_all(outgoing, mesh_axis, 0, 0), axis=dim)
 
 
 def rms_scale(values):
@@ -176,7 +181,7 @@
     arrived = lax.all_to_all(outbound, "sp", split_axis=0, concat_axis=0, tiled=True)
     item_count = arrived.shape[1]
     flat_rows = arrived.reshape(sp_count * item_count, D)
-    row_block = lax.all_gather(flat_rows, "tp", axis=0, tiled=True)
+    row_block = exchange_gather(flat_rows, "tp", 0)
     gate_pre = jnp.dot(row_block, expert_gate[0], preferred_element_type=jnp.float32)
     up_pre = jnp.dot(row_block, expert_up[0], preferred_element_type=jnp.float32)
     hidden = (jax.nn.silu(gate_pre) * up_pre).astype(jnp.bfloat16)

time: 452 us -> 606 us (1.34)
  blocking collectives: 157 us -> 370 us
  waiting for transfers between devices: 212 us -> 151 us
    all_to_all x0 -> x1, blocking collectives: none -> 213 us  [exchange_gather(): return jnp.concatenate(lax.all_to_all(outgoing, mesh_axis, 0, 0), axis=dim)]
    all_gather x1 -> x0, waiting for transfers between devices: 57.2 us -> none  [shards(): row_block = lax.all_gather(flat_rows, 'tp', axis=0, tiled=True)]
  transfers between devices with their start and end apart: 5 -> 4, of which waited for: 5 -> 4; matrix products, arithmetic and copies ran while one was open for 0% -> 0% of each run, Pallas kernels for 0% -> 0%
where the time goes in v1:
time: 606 us; the launch traced here: 605 us
  blocking collectives  370 us (61%)
  waiting for transfers between devices  151 us (25%)
  matrix products  28.7 us (5%)
  starting transfers between devices  14.3 us (2%)
  local copies, waits for them, and re-layouts  13.9 us (2%)
  between operations  13.8 us (2%)
  other arithmetic  12 us (2%)
    all_to_all x1, blocking collectives, exchange_gather(): return jnp.concatenate(lax.all_to_all(outgoing, mesh_axis, 0, 0), axis=dim)  213 us
    all_to_all x1, blocking collectives, shards(): lax.all_to_all(outbound, 'sp', split_axis=0, concat_axis=0, tiled=True)  157 us
    reduce_scatter x1, waiting for transfers between devices, shards(): lax.psum_scatter(jnp.dot(hidden, expert_down[0], preferred_element_type=j...  68.1 us
    all_gather x1, waiting for transfers between devices, shards(): key_piece = lax.all_gather(bundle, 'sp', axis=2, tiled=True)  61.9 us
    all_to_all x1, waiting for transfers between devices, shards(): lax.all_to_all(served, 'sp', split_axis=0, concat_axis=0, tiled=True)  15.1 us
    dot_general x1, matrix products, shards(): jnp.dot(hidden, expert_down[0], preferred_element_type=jnp.float32)  14.3 us
  transfers between devices with their start and end apart: 4, of which 4 were waited for; matrix products, arithmetic and copies ran while one was open for 0% of the time, Pallas kernels for 0%

profile of v1, /device:TPU:97, one launch (start us, length us, event | category | flops | bytes accessed | tf_op | source)
XLA Modules:
  0.0 604.8 jit_solution(11549392763498200258)
XLA Ops:
  6.6 1.6 fusion.21
  8.3 1.8 fusion.29
  10.1 0.9 fusion.40
  11.0 1.0 fusion.42
  12.0 1.0 fusion.41
  13.0 0.6 fusion.30
  13.7 0.3 fusion.74
  14.1 0.7 pad_maximum_fusion
  14.9 0.2 copy.34
  15.2 0.1 reshape.501
  15.5 0.2 reduce_window_sum.11
  15.7 0.2 select_reduce_fusion
  15.8 0.1 reduce_sum.105
  16.1 61.9 %all-gather.2.cloned.1.call-done = bf16[1,160,16384]{2,1,0:T(8,128)(2,1)} async-done(((bf16[1,160,1024]{2,1,0:T(8,128)(2,1)}), bf16[1,160,16384]{2,1,0:T(8,128)(2,1)}) %all-gather.2.cloned.1.call-update) | async-done | bytes 5242896 | tf_op jit(solution)/shard_map/all_gather | solution.py:119
  78.0 9.9 %while.18 = (s32[]{:T(128)}, f32[1,1024]{1,0:T(1,128)S(1)}, f32[1,1024]{1,0:T(1,128)S(1)}, f32[1,1024,64]{1,2,0:T(8,128)S(1)}, s32[]{:T(128)}, /*index=5*/bf16[1...) while((s32[]{:T(128)}, f32[1,1024]{1,0:T(1,128)S(1)}, ...), condition=%wide.region_8.9_spmd.clone, body=%wide.region_3.8_spmd.clone.sunk | while | flops 352456704 | bytes 30515560 | solution.py:154
  78.0 9.1 %conditional.3 = ((f32[1,1024]{1,0:T(1,128)S(1)}, f32[1,1024]{1,0:T(1,128)S(1)}, f32[1,1024,64]{1,2,0:T(8,128)S(1)})) conditional(s32[]{:T(128)} %convert_element_type.207, (f32[1,1024]{1,0:T(1,128)S(1)}, f32[1,1024]{1,0:T(1,128)S(1)}, f32[1,1024,64]{1,2,0:T(8,128)S(1)}) %tuple.54, (s32[]{:T(128)}, s32[]{:T(128)}, s32[]{:T(128)}, ...), branch_computations={%region_4.0_spmd, %region_5.7_spmd} | conditional | flops 352456704 | bytes 30511242 | solution.py:152
  78.0 2.0 fusion.2
  80.1 2.0 copy-done.1
  82.1 1.5 fusion.4
  83.7 3.5 fusion.10
  87.9 0.2 copy.41
  88.1 0.9 reshape.514
  89.0 7.8 %all-to-all-start = ((bf16[16,2,2048]{2,1,0:T(2,128)(2,1)}), bf16[16,2,2048]{2,1,0:T(2,128)(2,1)S(1)}, u32[]{:S(2)}, u32[]{:S(2)}) async-start(bf16[16,2,2048]{2,1,0:T(2,128)(2,1)} %reshape.514), calls=%async_computation | async-start | bytes 262144 | tf_op jit(solution)/shard_map/all_to_all | solution.py:158
  96.9 6.2 %all-to-all-done = bf16[16,2,2048]{2,1,0:T(2,128)(2,1)S(1)} async-done(((bf16[16,2,2048]{2,1,0:T(2,128)(2,1)}), bf16[16,2,2048]{2,1,0:T(2,128)(2,1)S(1)}, u32[]{:S(2)}, u32[]{:S(2)}) %all-to-all-start) | async-done | bytes 131104 | tf_op jit(solution)/shard_map/all_to_all | solution.py:158
  103.1 0.2 reshape.515
  103.3 0.2 fusion.32
  103.5 3.5 convert_bitcast_fusion
  107.1 0.8 convert_reduce_fusion
  107.8 0.2 copy-done.3
  108.0 0.2 multiply_reduce_fusion.1
  108.2 0.4 convolution_convert_fusion.1
  108.5 0.2 reshape.502
  108.8 156.9 %all_to_all.28 = bf16[16,9,2048]{2,1,0:T(8,128)(2,1)S(1)} all-to-all(bf16[16,9,2048]{2,1,0:T(8,128)(2,1)S(1)} %reshape.502), channel_id=1, replica_groups=mesh['sp'=16,'tp'=16] {'sp'}, dimensions={0} | all-to-all | bytes 1179648 | tf_op jit(solution)/shard_map/all_to_all | solution.py:181
  265.7 0.3 stack_reshape.2
  266.0 1.2 stack.3
  267.2 213.0 %all_to_all.29 = bf16[16,144,2048]{2,1,0:T(8,128)(2,1)S(1)} all-to-all(bf16[16,144,2048]{2,1,0:T(8,128)(2,1)S(1)} %stack.3), channel_id=1, replica_groups=mesh['sp'=16,'tp'=16] {'tp'}, dimensions={0} | all-to-all | bytes 18874368 | tf_op jit(solution)/shard_map/all_to_all | solution.py:18
  480.2 3.7 copy-done.2
  483.8 2.7 fusion.38
  486.5 14.3 %convolution_convert_fusion = bf16[2304,2048]{1,0:T(8,128)(2,1)} fusion(bf16[2304,2048]{1,0:T(8,128)(2,1)} %bitcast.85, f32[2304,128]{1,0:T(8,128)S(1)} %fusion.38, bf16[1,128,2048]{2,1,0:T(8,128)(2,1)S(1)} %copy-done, bf16[1,2048,128]{2,1,0:T(8,128)(2,1)S(1)} %copy-done.6), kind=kOutput, calls=%fused_computation.23 | convolution fusion | flops 2422407168 | bytes 21102592 | tf_op jit(solution)/shard_map/dot_general | solution.py:189
  500.8 68.1 %reduce-scatter.2.cloned.1.call-done = bf16[144,2048]{1,0:T(8,128)(2,1)} async-done(((bf16[2304,2048]{1,0:T(8,128)(2,1)}), bf16[144,2048]{1,0:T(8,128)(2,1)}) %reduce-scatter.2.cloned.1.call-update) | async-done | bytes 589840 | tf_op jit(solution)/shard_map/reduce_scatter | solution.py:188
  568.9 2.3 reshape.504
  571.2 6.5 %all-to-all-start.3 = ((bf16[16,9,2048]{2,1,0:T(8,128)(2,1)}), bf16[16,9,2048]{2,1,0:T(8,128)(2,1)S(1)}, u32[]{:S(2)}, u32[]{:S(2)}) async-start(bf16[16,9,2048]{2,1,0:T(8,128)(2,1)} %reshape.504), calls=%async_computation.4 | async-start | bytes 2097152 | tf_op jit(solution)/shard_map/all_to_all | solution.py:194
  578.2 15.1 %all-to-all-done.3 = bf16[16,9,2048]{2,1,0:T(8,128)(2,1)S(1)} async-done(((bf16[16,9,2048]{2,1,0:T(8,128)(2,1)}), bf16[16,9,2048]{2,1,0:T(8,128)(2,1)S(1)}, u32[]{:S(2)}, u32[]{:S(2)}) %all-to-all-start.3) | async-done | bytes 589856 | tf_op jit(solution)/shard_map/all_to_all | solution.py:194
  593.3 0.3 reshape.505
  593.5 0.9 gather_fusion
  594.5 0.3 gather.7
  594.8 2.3 multiply_reduce_fusion
  597.1 0.8 add_convert_fusion
  (95 shorter events, 1.6 us)
Async XLA Ops:
  6.5 480.0 %copy-start = (bf16[1,128,2048]{2,1,0:T(8,128)(2,1)S(1)}, bf16[1,128,2048]{2,1,0:T(8,128)(2,1)}, u32[]{:S(2)}) copy-start(bf16[1,128,2048]{2,1,0:T(8,128)(2,1)} %param.37) | copy-start | bytes 1572868
  6.5 6.4 %copy-start.4 = (bf16[1024,512]{1,0:T(8,128)(2,1)S(1)}, bf16[1024,512]{1,0:T(8,128)(2,1)}, u32[]{:S(2)}) copy-start(bf16[1024,512]{1,0:T(8,128)(2,1)} %param.22) | copy-start | bytes 3145732
  6.5 6.5 %copy-start.14 = (f32[512]{0:T(512)S(1)}, f32[512]{0:T(512)}, u32[]{:S(2)}) copy-start(f32[512]{0:T(512)} %param.24) | copy-start | bytes 6148
  6.5 7.0 %copy-start.5 = (bf16[1024,96]{0,1:T(8,128)(2,1)S(1)}, bf16[1024,96]{0,1:T(8,128)(2,1)}, u32[]{:S(2)}) copy-start(bf16[1024,96]{0,1:T(8,128)(2,1)} %param.21) | copy-start | bytes 589828
  6.5 6.5 %copy-start.13 = (bf16[512,64]{0,1:T(8,128)(2,1)S(1)}, bf16[512,64]{0,1:T(8,128)(2,1)}, u32[]{:S(2)}) copy-start(bf16[512,64]{0,1:T(8,128)(2,1)} %param.26) | copy-start | bytes 196612
  6.5 7.0 %copy-start.11 = (f32[96]{0:T(128)S(1)}, f32[96]{0:T(128)}, u32[]{:S(2)}) copy-start(f32[96]{0:T(128)} %param.27) | copy-start | bytes 1156
  6.6 71.4 %all-gather.2.cloned.1.call-start = ((), (), s32[]{:S(2)}) async-start(), calls=%async_computation.5 | async-start | bytes 5570560 | tf_op jit(solution)/shard_map/all_gather | solution.py:119
  8.3 6.8 %copy-start.9 = (f32[1024]{0:T(1024)S(1)}, f32[1024]{0:T(1024)}, u32[]{:S(2)}) copy-start(f32[1024]{0:T(1024)} %param.29) | copy-start | bytes 12292
  8.3 6.9 %copy-start.7 = (s32[64,2]{0,1:T(2,128)S(1)}, s32[64,2]{0,1:T(2,128)}, u32[]{:S(2)}) copy-start(s32[64,2]{0,1:T(2,128)} %param.33) | copy-start | bytes 1540
  80.1 2.0 copy-start.1
  89.0 14.1 %all-to-all-start = ((bf16[16,2,2048]{2,1,0:T(2,128)(2,1)}), bf16[16,2,2048]{2,1,0:T(2,128)(2,1)S(1)}, u32[]{:S(2)}, u32[]{:S(2)}) async-start(bf16[16,2,2048]{2,1,0:T(2,128)(2,1)} %reshape.514), calls=%async_computation | async-start | bytes 262144 | tf_op jit(solution)/shard_map/all_to_all | solution.py:158
  96.8 472.1 %reduce-scatter.2.cloned.1.call-start = ((), (), s32[]{:S(2)}) async-start(), calls=%async_computation.6 | async-start | bytes 10027008 | tf_op jit(solution)/shard_map/reduce_scatter | solution.py:188
  107.0 1.0 copy-start.3
  107.0 1.1 copy-start.8
  267.2 216.6 %copy-start.12 = (bf16[1,2048,128]{2,1,0:T(8,128)(2,1)S(1)}, bf16[1,2048,128]{2,1,0:T(8,128)(2,1)}, u32[]{:S(2)}) copy-start(bf16[1,2048,128]{2,1,0:T(8,128)(2,1)} %param.35) | copy-start | bytes 1572868
  480.2 3.7 copy-start.2
  483.8 2.7 copy-start.6
  500.8 77.3 %copy-start.10 = (f32[64,2]{0,1:T(2,128)S(1)}, f32[64,2]{0,1:T(2,128)}, u32[]{:S(2)}) copy-start(f32[64,2]{0,1:T(2,128)} %param.34) | copy-start | bytes 1540
  571.2 22.1 %all-to-all-start.3 = ((bf16[16,9,2048]{2,1,0:T(8,128)(2,1)}), bf16[16,9,2048]{2,1,0:T(8,128)(2,1)S(1)}, u32[]{:S(2)}, u32[]{:S(2)}) async-start(bf16[16,9,2048]{2,1,0:T(8,128)(2,1)} %reshape.504), calls=%async_computation.4 | async-start | bytes 2097152 | tf_op jit(solution)/shard_map/all_to_all | solution.py:194
Sparse Core Ops, SparseCore 0:
  14.9 62.9 all-gather.1
  500.9 67.9 reduce-scatter.1
